TPU v7x, 512 devices: a whole 4x8x8 slice. The times are simulated.
512 devices in a mesh: sp: 64 (over z, y), tp: 8 (over x, core).
Axes of the slice: x: 4, y: 8, z: 8, core: 2. Of those that a mesh axis runs over, the one named last changes fastest.
Arguments:
- queries: bfloat16 [32768, 2048], P('sp', 'tp'), may hold values from -14 to 14
- key_states: bfloat16 [32768, 512], P('sp', 'tp'), may hold values from -14 to 14
- value_states: bfloat16 [32768, 512], P('sp', 'tp'), may hold values from -6 to 6
- sink_logits: float32 [32], P('tp'), may hold values from 0 to 5
- out_weight: bfloat16 [2048, 2048], P('tp'), may hold values from -0.125 to 0.125
- residual: bfloat16 [32768, 2048], P(('sp', 'tp')), may hold values from -6 to 6
- gain_attn: float32 [2048], replicated, may hold values from 0.1 to 1.9
- gain_before: float32 [2048], replicated, may hold values from 0.1 to 1.9
- gain_after: float32 [2048], replicated, may hold values from 0.1 to 1.9
- gate_weight: bfloat16 [2048, 5632], P('sp', 'tp'), may hold values from -0.125 to 0.125
- value_weight: bfloat16 [2048, 5632], P('sp', 'tp'), may hold values from -0.125 to 0.125
- gate_taps: float32 [3, 5632], P(None, 'tp'), may hold values from -3 to 3
- value_taps: float32 [3, 5632], P(None, 'tp'), may hold values from -3 to 3
- down_weight: bfloat16 [5632, 2048], P('tp', 'sp'), may hold values from -0.078125 to 0.078125
Outputs:
- layer_out: bfloat16 [32768, 2048], P(('sp', 'tp'))
All inputs are finite; a program needn't handle non-finite values.
Results may differ from a plain program's by a relative error of at most 0.018.
Values may be sent and summed in bfloat16 or wider, within the bound.
A program may use at most 64 MiB of HBM per device.

v0:
```python
import jax
import jax.numpy as jnp
from jax import lax
from jax.sharding import PartitionSpec as P

HD = 64
WINDOW = 128


NEG_FILL = -1e30


def passed_along(block, axis, distance):
    devices = range(lax.axis_size(axis))
    route = [(i - distance, i) for i in devices if i - distance in devices]
    return lax.ppermute(block, axis, route)


def in_blocks(shard, dim, peers):
    before, after = (shard.shape[:dim], shard.shape[dim + 1 :])
    return jnp.moveaxis(shard.reshape(*before, peers, -1, *after), dim, 0)


def sum_at_owner(shard, axis, dim):
    peers = lax.axis_size(axis)
    pieces = lax.all_to_all(in_blocks(shard, dim, peers), axis, 0, 0, tiled=True)
    return jnp.sum(pieces.astype(jnp.float32), axis=0)


def in_order(pieces, dim):
    pieces = jnp.moveaxis(pieces, 0, dim)
    lengths = pieces.shape
    return pieces.reshape(*lengths[:dim], lengths[dim] * lengths[dim + 1], *lengths[dim + 2 :])


def sent_to_all(shard, axis):
    copies = jnp.broadcast_to(shard, (lax.axis_size(axis), *shard.shape))
    return lax.all_to_all(copies, axis, split_axis=0, concat_axis=0, tiled=True)


def gather_directly(shard, axis, dim):
    return in_order(sent_to_all(shard, axis), dim)


def in_one_piece(arrays, axis, dim, along):
    widths = [a.shape[along] for a in arrays]
    both = jnp.concatenate(arrays, axis=along)
    filled = lax.all_gather(both, axis, axis=dim, tiled=True)
    return tuple(jnp.split(filled, [sum(widths[:k]) for k in range(1, len(widths))], axis=along))


def rms_scale(matrix):
    return matrix * lax.rsqrt(jnp.mean(matrix * matrix, axis=-1, keepdims=True) + 1e-06)


def attention_local(queries, key_states, value_states, sink_logits):
    length = queries.shape[0]
    blocks = length // WINDOW
    kv_local = key_states.shape[1] // HD
    grouping = queries.shape[1] // key_states.shape[1]
    earlier_keys, earlier_values = passed_along(
        (key_states[length - WINDOW :], value_states[length - WINDOW :]), "sp", 1
    )
    keys_ext = jnp.concatenate([earlier_keys, key_states], axis=0).reshape(
        blocks + 1, WINDOW, kv_local, HD
    )
    values_ext = jnp.concatenate([earlier_values, value_states], axis=0).reshape(
        blocks + 1, WINDOW, kv_local, HD
    )
    key_blocks = jnp.concatenate([keys_ext[:-1], keys_ext[1:]], axis=1)
    value_blocks = jnp.concatenate([values_ext[:-1], values_ext[1:]], axis=1)
    query_blocks = queries.reshape(blocks, WINDOW, kv_local, grouping, HD)
    offset = lax.axis_index("sp") * length
    qpos = (offset + jnp.arange(length, dtype=jnp.int32)).reshape(blocks, WINDOW)
    kpos = jnp.concatenate([qpos - WINDOW, qpos], axis=1)
    visible = (
        (kpos[:, None, :] <= qpos[:, :, None])
        & (qpos[:, :, None] - kpos[:, None, :] < WINDOW)
        & (kpos[:, None, :] >= 0)
    )
    scores = jnp.einsum(
        "nqhgd,nkhd->nhgqk", query_blocks, key_blocks, preferred_element_type=jnp.float32
    ) * HD ** (-0.5)
    scores = jnp.where(visible[:, None, None], scores, NEG_FILL)
    sink_col = sink_logits.reshape(kv_local, grouping)[None, :, :, None]
    top = jnp.maximum(jnp.max(scores, axis=-1), sink_col)
    expo = jnp.exp(scores - top[..., None])
    total = jnp.sum(expo, axis=-1) + jnp.exp(sink_col - top)
    probs = (expo / total[..., None]).astype(jnp.bfloat16)
    result = jnp.einsum(
        "nhgqk,nkhd->nqhgd", probs, value_blocks, preferred_element_type=jnp.float32
    )
    return result.astype(jnp.bfloat16).reshape(length, queries.shape[1])


def causal_local(upward, earlier, kernel):
    length = upward.shape[0]
    padded = jnp.concatenate([earlier, upward], axis=0).astype(jnp.float32)
    result = jnp.zeros(upward.shape, jnp.float32)
    for tap_index in range(kernel.shape[0]):
        result = result + kernel[tap_index][None, :] * padded[tap_index : tap_index + length]
    return result


def on_device(
    queries,
    key_states,
    value_states,
    sink_logits,
    out_weight,
    residual,
    gain_attn,
    gain_before,
    gain_after,
    gate_weight,
    value_weight,
    gate_taps,
    value_taps,
    down_weight,
):
    length = queries.shape[0]
    attended = attention_local(queries, key_states, value_states, sink_logits)
    selected = attended
    attn_proj = sum_at_owner(
        jnp.dot(selected, out_weight, preferred_element_type=jnp.float32).astype(jnp.bfloat16),
        "tp",
        0,
    )
    middle = residual.astype(jnp.float32) + rms_scale(attn_proj) * gain_attn
    normed = (rms_scale(middle) * gain_before).astype(jnp.bfloat16)
    whole_rows = gather_directly(normed, "tp", 0)
    gate_full, value_full = in_one_piece((gate_weight, value_weight), "sp", 0, 1)
    gate_up = jnp.dot(whole_rows, gate_full, preferred_element_type=jnp.float32).astype(
        jnp.bfloat16
    )
    value_up = jnp.dot(whole_rows, value_full, preferred_element_type=jnp.float32).astype(
        jnp.bfloat16
    )
    reach = gate_taps.shape[0] - 1
    gate_before, value_before = passed_along(
        (gate_up[length - reach :], value_up[length - reach :]), "sp", 1
    )
    gate_conv = causal_local(gate_up, gate_before, gate_taps)
    value_conv = causal_local(value_up, value_before, value_taps)
    hidden = (jax.nn.silu(gate_conv) * value_conv).astype(jnp.bfloat16)
    down_whole = lax.all_gather(down_weight, "sp", axis=1, tiled=True)
    selected = hidden
    down = sum_at_owner(
        jnp.dot(selected, down_whole, preferred_element_type=jnp.float32).astype(jnp.bfloat16),
        "tp",
        0,
    )
    return (middle + rms_scale(down) * gain_after).astype(jnp.bfloat16)


def solution(mesh):
    in_specs = (
        P("sp", "tp"),
        P("sp", "tp"),
        P("sp", "tp"),
        P("tp"),
        P("tp", None),
        P(("sp", "tp"), None),
        P(),
        P(),
        P(),
        P("sp", "tp"),
        P("sp", "tp"),
        P(None, "tp"),
        P(None, "tp"),
        P("tp", "sp"),
    )
    out_specs = P(("sp", "tp"), None)
    return jax.shard_map(
        on_device, mesh=mesh, in_specs=in_specs, out_specs=out_specs, check_vma=False
    )
```

profile of v0, /device:TPU:1, one launch (start us, length us, event | category | flops | bytes accessed | tf_op | source)
XLA Modules:
  0.0 238.2 jit_solution(13050096968348563992)
XLA Ops:
  6.5 0.0 copy-start
  6.5 0.0 copy-start.2
  6.5 0.0 all-gather.3.cloned.1.call-start
  6.5 1.6 pad_maximum_fusion
  8.2 0.0 all-gather.3.cloned.1.call-update
  8.2 0.7 slice.72
  8.9 4.0 %collective-permute-start.1 = (bf16[128,64]{0,1:T(8,128)(2,1)S(1)}, bf16[128,64]{0,1:T(8,128)(2,1)S(1)}, u32[]{:S(2)}, u32[]{:S(2)}) collective-permute-start(bf16[128,64]{0,1:T(8,128)(2,1)S(1)} %slice.72), channel_id=1, source_target_pairs={{0,8},{8,16},{16,24},{24,32},{32,40},{40,48},{48,56},{56,64},{64,7... | collective-permute-start | bytes 49160 | tf_op jit(solution)/shard_map/ppermute | solution.py:16
  13.0 0.7 slice.68
  13.7 3.2 %collective-permute-start = (bf16[128,64]{0,1:T(8,128)(2,1)S(1)}, bf16[128,64]{0,1:T(8,128)(2,1)S(1)}, u32[]{:S(2)}, u32[]{:S(2)}) collective-permute-start(bf16[128,64]{0,1:T(8,128)(2,1)S(1)} %slice.68), channel_id=1, source_target_pairs={{0,8},{8,16},{16,24},{24,32},{32,40},{40,48},{48,56},{56,64},{64,7... | collective-permute-start | bytes 49160 | tf_op jit(solution)/shard_map/ppermute | solution.py:16
  16.9 0.3 fusion.29
  17.3 0.9 slice.75
  18.1 0.9 slice.71
  19.0 1.2 reshape.136
  20.2 0.0 copy-start.8
  20.3 0.0 collective-permute-done.1
  20.3 0.8 pad_maximum_fusion.1
  21.2 0.0 collective-permute-done
  21.2 0.0 copy-done.2
  21.2 0.5 fusion.39
  21.8 0.0 copy-done.8
  21.8 0.1 broadcast_maximum_fusion
  21.9 0.3 fusion.4
  22.2 0.1 exponential_add_fusion
  22.3 0.5 fusion.17
  22.8 0.2 copy.24
  23.0 0.0 copy-done
  23.0 2.1 convolution_convert_fusion
  25.1 6.4 %all-to-all-start = ((bf16[8,64,2048]{2,1,0:T(8,128)(2,1)}), bf16[8,64,2048]{2,1,0:T(8,128)(2,1)}, u32[]{:S(2)}, u32[]{:S(2)}) async-start(bf16[8,64,2048]{2,1,0:T(8,128)(2,1)} %bitcast.11), calls=%async_computation | async-start | bytes 4194304 | tf_op jit(solution)/shard_map/all_to_all | solution.py:26
  31.5 0.0 copy-start.1
  31.5 0.0 all-gather.5.cloned.1.call-start
  31.6 0.7 all-gather.5.cloned.1.call-update
  32.3 25.6 %all-to-all-done = bf16[8,64,2048]{2,1,0:T(8,128)(2,1)} async-done(((bf16[8,64,2048]{2,1,0:T(8,128)(2,1)}), bf16[8,64,2048]{2,1,0:T(8,128)(2,1)}, u32[]{:S(2)}, u32[]{:S(2)}) %all-to-all-start) | async-done | bytes 2097184 | tf_op jit(solution)/shard_map/all_to_all | solution.py:26
  57.9 2.0 convert_reduce_fusion.1
  59.9 0.1 multiply_reduce_fusion.2
  60.0 0.0 copy-done.1
  60.0 0.0 copy-done.3
  60.0 0.3 multiply_reduce_fusion.1
  60.3 0.0 copy-done.4
  60.3 0.2 multiply_convert_fusion
  60.5 1.6 broadcast_in_dim.16
  62.1 5.3 %all-to-all-start.1 = ((bf16[8,64,2048]{2,1,0:T(8,128)(2,1)}), bf16[8,64,2048]{2,1,0:T(8,128)(2,1)}, u32[]{:S(2)}, u32[]{:S(2)}) async-start(bf16[8,64,2048]{2,1,0:T(8,128)(2,1)} %broadcast_in_dim.16), calls=%async_computation.1 | async-start | bytes 4194304 | tf_op jit(solution)/shard_map/all_to_all | solution.py:38
  67.5 0.0 copy-done.6
  67.5 0.0 copy-done.7
  67.5 0.1 slice_reduce_fusion.2
  67.6 26.3 %all-to-all-done.1 = bf16[8,64,2048]{2,1,0:T(8,128)(2,1)} async-done(((bf16[8,64,2048]{2,1,0:T(8,128)(2,1)}), bf16[8,64,2048]{2,1,0:T(8,128)(2,1)}, u32[]{:S(2)}, u32[]{:S(2)}) %all-to-all-start.1) | async-done | bytes 2097184 | tf_op jit(solution)/shard_map/all_to_all | solution.py:38
  93.8 8.4 %all-gather.3.cloned.1.call-done = bf16[2048,1408]{1,0:T(8,128)(2,1)} async-done(((bf16[32,1408]{1,0:T(8,128)(2,1)}), bf16[2048,1408]{1,0:T(8,128)(2,1)}) %all-gather.3.cloned.1.call-update) | async-done | bytes 5767184 | tf_op jit(solution)/shard_map/all_gather | solution.py:48
  102.2 4.4 %fusion.11 = bf16[512,704]{0,1:T(8,128)(2,1)S(1)} fusion(bf16[512,2048]{1,0:T(8,128)(2,1)} %bitcast.12, bf16[2048,1408]{1,0:T(8,128)(2,1)} %all-gather.3.cloned.1.call-done), kind=kOutput, calls=%fused_computation.24 | convolution fusion | flops 1476755456 | bytes 5963776 | tf_op jit(solution)/shard_map/dot_general | solution.py:133
  106.6 0.1 slice.90
  106.7 2.7 %collective-permute-start.2 = (bf16[2,704]{0,1:T(8,128)(2,1)S(1)}, bf16[2,704]{0,1:T(8,128)(2,1)S(1)}, u32[]{:S(2)}, u32[]{:S(2)}) collective-permute-start(bf16[2,704]{0,1:T(8,128)(2,1)S(1)} %slice.90), channel_id=1, source_target_pairs={{0,8},{8,16},{16,24},{24,32},{32,40},{40,48},{48,56},{56,64},{64,7... | collective-permute-start | bytes 8456 | tf_op jit(solution)/shard_map/ppermute | solution.py:16
  109.4 0.0 copy-done.9
  109.4 4.5 %fusion.14 = bf16[512,704]{0,1:T(8,128)(2,1)S(1)} fusion(bf16[512,2048]{1,0:T(8,128)(2,1)} %bitcast.12, bf16[2048,1408]{1,0:T(8,128)(2,1)S(1)} %copy-done.9), kind=kOutput, calls=%fused_computation.25 | convolution fusion | flops 1476755456 | bytes 5963776 | tf_op jit(solution)/shard_map/dot_general | solution.py:136
  113.9 0.1 slice.94
  114.0 3.7 %collective-permute-start.3 = (bf16[2,704]{0,1:T(8,128)(2,1)S(1)}, bf16[2,704]{0,1:T(8,128)(2,1)S(1)}, u32[]{:S(2)}, u32[]{:S(2)}) collective-permute-start(bf16[2,704]{0,1:T(8,128)(2,1)S(1)} %slice.94), channel_id=1, source_target_pairs={{0,8},{8,16},{16,24},{24,32},{32,40},{40,48},{48,56},{56,64},{64,7... | collective-permute-start | bytes 8456 | tf_op jit(solution)/shard_map/ppermute | solution.py:16
  117.7 0.0 collective-permute-done.2
  117.7 1.6 maximum_convert_fusion
  119.3 0.6 collective-permute-done.3
  119.9 1.6 maximum_convert_fusion.1
  121.5 64.6 %all-gather.5.cloned.1.call-done = bf16[704,2048]{0,1:T(8,128)(2,1)} async-done(((bf16[704,32]{0,1:T(8,128)(2,1)}), bf16[704,2048]{0,1:T(8,128)(2,1)}) %all-gather.5.cloned.1.call-update) | async-done | bytes 2883600 | tf_op jit(solution)/shard_map/all_gather | solution.py:146
  186.1 9.1 %convolution_convert_fusion.1 = bf16[512,2048]{1,0:T(8,128)(2,1)S(1)} fusion(bf16[704,2048]{0,1:T(8,128)(2,1)} %all-gather.5.cloned.1.call-done, f32[514,704]{0,1:T(8,128)} %maximum_convert_fusion.1, f32[514,704]{0,1:T(8,128)} %maximum_convert_fusion, f32[704]{0:T(1024)S(1)} %get-tuple-element.9, f32[704]{0:T(1024)S(1)} %get-tuple-element.10, ...), kind=kOutput, calls=%fused_computation.7 | convolution fusion | flops 1483210752 | bytes 13910528 | tf_op jit(solution)/shard_map/dot_general | solution.py:149
  195.2 34.6 %all_to_all.15 = bf16[8,64,2048]{2,1,0:T(8,128)(2,1)S(1)} all-to-all(bf16[8,64,2048]{2,1,0:T(8,128)(2,1)S(1)} %bitcast.47), channel_id=1, replica_groups=mesh['sp'=64,'tp'=8] {'tp'}, dimensions={0} | all-to-all | bytes 4194304 | tf_op jit(solution)/shard_map/all_to_all | solution.py:26
  229.8 0.4 convert_reduce_fusion
  230.1 0.1 multiply_reduce_fusion
  230.3 0.2 copy-done.5
  230.5 0.9 add_convert_fusion
  (20 shorter events, 0.2 us)
Async XLA Ops:
  6.5 16.4 %copy-start = (bf16[256,2048]{1,0:T(8,128)(2,1)S(1)}, bf16[256,2048]{1,0:T(8,128)(2,1)}, u32[]{:S(2)}) copy-start(bf16[256,2048]{1,0:T(8,128)(2,1)} %param.18) | copy-start | bytes 3145732
  6.5 14.6 %copy-start.2 = (bf16[512,64]{0,1:T(8,128)(2,1)S(1)}, bf16[512,64]{0,1:T(8,128)(2,1)}, u32[]{:S(2)}) copy-start(bf16[512,64]{0,1:T(8,128)(2,1)} %param.16) | copy-start | bytes 196612
  6.5 95.7 %all-gather.3.cloned.1.call-start = ((), (), s32[]{:S(2)}) async-start(), calls=%async_computation.3 | async-start | bytes 5857280 | tf_op jit(solution)/shard_map/all_gather | solution.py:48
  8.9 11.4 %collective-permute-start.1 = (bf16[128,64]{0,1:T(8,128)(2,1)S(1)}, bf16[128,64]{0,1:T(8,128)(2,1)S(1)}, u32[]{:S(2)}, u32[]{:S(2)}) collective-permute-start(bf16[128,64]{0,1:T(8,128)(2,1)S(1)} %slice.72), channel_id=1, source_target_pairs={{0,8},{8,16},{16,24},{24,32},{32,40},{40,48},{48,56},{56,64},{64,7... | collective-permute-start | bytes 49160 | tf_op jit(solution)/shard_map/ppermute | solution.py:16
  13.7 7.5 %collective-permute-start = (bf16[128,64]{0,1:T(8,128)(2,1)S(1)}, bf16[128,64]{0,1:T(8,128)(2,1)S(1)}, u32[]{:S(2)}, u32[]{:S(2)}) collective-permute-start(bf16[128,64]{0,1:T(8,128)(2,1)S(1)} %slice.68), channel_id=1, source_target_pairs={{0,8},{8,16},{16,24},{24,32},{32,40},{40,48},{48,56},{56,64},{64,7... | collective-permute-start | bytes 49160 | tf_op jit(solution)/shard_map/ppermute | solution.py:16
  20.2 1.5 copy-start.8
  25.1 32.8 %all-to-all-start = ((bf16[8,64,2048]{2,1,0:T(8,128)(2,1)}), bf16[8,64,2048]{2,1,0:T(8,128)(2,1)}, u32[]{:S(2)}, u32[]{:S(2)}) async-start(bf16[8,64,2048]{2,1,0:T(8,128)(2,1)} %bitcast.11), calls=%async_computation | async-start | bytes 4194304 | tf_op jit(solution)/shard_map/all_to_all | solution.py:26
  31.5 28.5 %copy-start.1 = (bf16[64,2048]{1,0:T(8,128)(2,1)S(1)}, bf16[64,2048]{1,0:T(8,128)(2,1)}, u32[]{:S(2)}) copy-start(bf16[64,2048]{1,0:T(8,128)(2,1)} %param.19) | copy-start | bytes 786436
  31.5 28.5 %copy-start.3 = (f32[2048]{0:T(1024)S(1)}, f32[2048]{0:T(1024)}, u32[]{:S(2)}) copy-start(f32[2048]{0:T(1024)} %param.20) | copy-start | bytes 24580
  31.5 28.8 %copy-start.4 = (f32[2048]{0:T(1024)S(1)}, f32[2048]{0:T(1024)}, u32[]{:S(2)}) copy-start(f32[2048]{0:T(1024)} %param.21) | copy-start | bytes 24580
  31.5 154.6 %all-gather.5.cloned.1.call-start = ((), (), s32[]{:S(2)}) async-start(), calls=%async_computation.4 | async-start | bytes 3194880 | tf_op jit(solution)/shard_map/all_gather | solution.py:146
  62.1 5.3 %copy-start.6 = (f32[3,704]{1,0:T(4,128)S(1)}, f32[3,704]{1,0:T(4,128)}, u32[]{:S(2)}) copy-start(f32[3,704]{1,0:T(4,128)} %param.26) | copy-start | bytes 25348
  62.1 5.3 %copy-start.7 = (f32[3,704]{1,0:T(4,128)S(1)}, f32[3,704]{1,0:T(4,128)}, u32[]{:S(2)}) copy-start(f32[3,704]{1,0:T(4,128)} %param.25) | copy-start | bytes 25348
  62.1 31.7 %all-to-all-start.1 = ((bf16[8,64,2048]{2,1,0:T(8,128)(2,1)}), bf16[8,64,2048]{2,1,0:T(8,128)(2,1)}, u32[]{:S(2)}, u32[]{:S(2)}) async-start(bf16[8,64,2048]{2,1,0:T(8,128)(2,1)} %broadcast_in_dim.16), calls=%async_computation.1 | async-start | bytes 4194304 | tf_op jit(solution)/shard_map/all_to_all | solution.py:38
  102.2 7.2 %copy-start.9 = (bf16[2048,1408]{1,0:T(8,128)(2,1)S(1)}, bf16[2048,1408]{1,0:T(8,128)(2,1)}, u32[]{:S(2)}) copy-start(bf16[2048,1408]{1,0:T(8,128)(2,1)} %all-gather.3.cloned.1.call-done) | copy-start | bytes 17301508
  106.7 11.0 %collective-permute-start.2 = (bf16[2,704]{0,1:T(8,128)(2,1)S(1)}, bf16[2,704]{0,1:T(8,128)(2,1)S(1)}, u32[]{:S(2)}, u32[]{:S(2)}) collective-permute-start(bf16[2,704]{0,1:T(8,128)(2,1)S(1)} %slice.90), channel_id=1, source_target_pairs={{0,8},{8,16},{16,24},{24,32},{32,40},{40,48},{48,56},{56,64},{64,7... | collective-permute-start | bytes 8456 | tf_op jit(solution)/shard_map/ppermute | solution.py:16
  114.0 5.9 %collective-permute-start.3 = (bf16[2,704]{0,1:T(8,128)(2,1)S(1)}, bf16[2,704]{0,1:T(8,128)(2,1)S(1)}, u32[]{:S(2)}, u32[]{:S(2)}) collective-permute-start(bf16[2,704]{0,1:T(8,128)(2,1)S(1)} %slice.94), channel_id=1, source_target_pairs={{0,8},{8,16},{16,24},{24,32},{32,40},{40,48},{48,56},{56,64},{64,7... | collective-permute-start | bytes 8456 | tf_op jit(solution)/shard_map/ppermute | solution.py:16
  229.8 0.7 copy-start.5
Sparse Core Ops, SparseCore 0:
  10.3 91.8 all-gather.2
  105.2 80.8 all-gather.4
where the time goes:
time: 239 us; the launch traced here: 238 us
  waiting for transfers between devices  126 us (53%)
  blocking collectives  34.6 us (14%)
  starting transfers between devices  25.4 us (11%)
  matrix products  21 us (9%)
  between operations  13.7 us (6%)
  other arithmetic  10.6 us (4%)
  local copies, waits for them, and re-layouts  6.82 us (3%)
    all_gather x1, waiting for transfers between devices, on_device(): down_whole = lax.all_gather(down_weight, 'sp', axis=1, tiled=True)  64.6 us
    all_to_all x1, blocking collectives, sum_at_owner(): lax.all_to_all(in_blocks(shard, dim, peers), axis, 0, 0, tiled=True)  34.6 us
    all_to_all x1, waiting for transfers between devices, sent_to_all(): return lax.all_to_all(copies, axis, split_axis=0, concat_axis=0, tiled=True)  26.3 us
    all_to_all x1, waiting for transfers between devices, sum_at_owner(): lax.all_to_all(in_blocks(shard, dim, peers), axis, 0, 0, tiled=True)  25.6 us
    ppermute x4, starting transfers between devices, passed_along(): return lax.ppermute(block, axis, route)  13.5 us
    dot_general x1, matrix products, on_device(): jnp.dot(selected, down_whole, preferred_element_type=jnp.float32)  9.1 us
    all_gather x1, waiting for transfers between devices, in_one_piece(): filled = lax.all_gather(both, axis, axis=dim, tiled=True)  8.4 us
    all_to_all x1, starting transfers between devices, sum_at_owner(): lax.all_to_all(in_blocks(shard, dim, peers), axis, 0, 0, tiled=True)  6.45 us
  transfers between devices with their start and end apart: 8, of which 5 were waited for; matrix products, arithmetic and copies ran while one was open for 11% of the time, Pallas kernels for 0%

commit v1 on v0

v1 whole, which is shorter than its diff:
```python
import jax
import jax.numpy as jnp
from jax import lax
from jax.experimental import pallas as pl
from jax.experimental.pallas import tpu as pltpu
from jax.sharding import PartitionSpec as P

HD = 64
WINDOW = 128
NEG_FILL = -1e30
MESH = pl.DeviceIdType.MESH
F32 = jnp.float32
BF16 = jnp.bfloat16
NT = (((1,), (1,)), ((), ()))


def rms_scale(matrix):
    return matrix * lax.rsqrt(jnp.mean(matrix * matrix, axis=-1, keepdims=True) + 1e-06)


def kernel(
    q_ref, kt_ref, vt_ref, sink_ref, ow_ref, res_ref, ga_ref, gb_ref, gc_ref,
    gw_ref, vw_ref, gt_ref, vt2_ref, dw_ref,
    out_ref,
    gv, dn, kvx, att, x_all, up, hid, mid,
    p_own, p_sib, r_sib, s_x, r_x,
    f_own, f_sib, g_sib, t_x, u_x,
    rp1, rp2, ssem, kv_sem, up_ss, up_rs,
    a_ss, a_rs, ax_ss, ax_rs, b_ss, b_rs, bx_ss, bx_rs, g_ss, g_rs,
):
    sp = lax.axis_index("sp")
    tp = lax.axis_index("tp")
    z, y = sp // 8, sp % 8
    x, c = tp // 2, tp % 2

    def at(zz, yy):
        return (zz % 8) * 8 + yy % 8

    def tp_at(xx, cc):
        return (xx % 4) * 2 + cc

    nxt, prv = ((sp + 1) % 64, tp), ((sp + 63) % 64, tp)
    sib = (sp, tp_at(x, 1 - c))
    xp, xm = (sp, tp_at(x + 1, c)), (sp, tp_at(x + 3, c))
    zn = ((at(z + 1, y), tp), (at(z + 7, y), tp))
    yn = ((at(z, y + 1), tp), (at(z, y + 7), tp))

    barrier = pltpu.get_barrier_semaphore()
    for dev in (nxt, prv, sib, xp, xm, *zn, *yn):
        pl.semaphore_signal(barrier, inc=1, device_id=dev, device_id_type=MESH)

    def remote(src, dst, ss, rs, dev):
        return pltpu.make_async_remote_copy(
            src_ref=src, dst_ref=dst, send_sem=ss, recv_sem=rs, device_id=dev, device_id_type=MESH
        )

    for h in range(2):
        rows = slice(16 * h, 16 * h + 16)
        for k in range(5):
            cols = slice(128 * k, 128 * k + 128)
            gv[z, y, h, :, 256 * k : 256 * k + 128] = gw_ref[rows, cols]
            gv[z, y, h, :, 256 * k + 128 : 256 * k + 256] = vw_ref[rows, cols]
            dn[z, y, h, :, cols] = dw_ref[rows, cols]
        gv[z, y, h, :, 1280:1408] = jnp.concatenate(
            [gw_ref[rows, 640:704].astype(F32), vw_ref[rows, 640:704].astype(F32)], axis=1
        ).astype(BF16)
        dn[z, y, h, :, 640:768] = jnp.concatenate(
            [dw_ref[rows, 640:704].astype(F32), jnp.zeros((16, 64), F32)], axis=1
        ).astype(BF16)
    kvx[0, :, 128:640] = kt_ref[...]
    kvx[1, :, 128:640] = vt_ref[...]

    pl.semaphore_wait(barrier, 9)

    def gather_steps(ps, buf):
        first = (y, z)
        second = (z, y)
        fdev = (yn, zn)
        sdev = (zn, yn)

        def item(h, f, s):
            f, s = f % 8, s % 8
            return buf.at[s, f, 0] if h == 0 else buf.at[f, s, 1]

        def batch(h, b, s):
            s = s % 8
            return buf.at[s, pl.ds(4 * b, 4), 0] if h == 0 else buf.at[pl.ds(4 * b, 4), s, 1]

        def send_first(h, d, k):
            f, s = first[h], second[h]
            ref = item(h, f + 9 - k if d == 0 else f + k - 1, s)
            remote(ref, ref, ssem.at[ps, h, d, 0], rp1.at[ps, h, d, k - 1], fdev[h][d]).start()

        def wait_first(h, d, k):
            f, s = first[h], second[h]
            ref = item(h, f + 8 - k if d == 0 else f + k, s)
            remote(ref, ref, ssem.at[ps, h, d, 0], rp1.at[ps, h, d, k - 1], fdev[h][d]).wait_recv()
            return f + 8 - k if d == 0 else f + k

        def send_own_group(h, f):
            f = f % 8
            ref = item(h, f, second[h])
            for d in range(2):
                remote(
                    ref, ref, ssem.at[ps, h, d, 1], rp2.at[ps, h, d, 0, f // 4], sdev[h][d]
                ).start()

        def group(h, d, k):
            return second[h] + 8 - k if d == 0 else second[h] + k

        def wait_second(h, d, k, b):
            ref = batch(h, b, group(h, d, k))
            remote(
                ref, ref, ssem.at[ps, h, d, 1], rp2.at[ps, h, d, k - 1, b], sdev[h][d]
            ).wait_recv()

        def forward(h, d, k, b):
            ref = batch(h, b, group(h, d, k))
            remote(
                ref, ref, ssem.at[ps, h, d, k + 1], rp2.at[ps, h, d, k, b], sdev[h][d]
            ).start()

        def step_own():
            for h in range(2):
                for d in range(2):
                    send_first(h, d, 1)
            for h in range(2):
                send_own_group(h, first[h])

        def step_first(k):
            def run():
                for d in range(2 if k < 4 else 1):
                    for h in range(2):
                        f = wait_first(h, d, k)
                        if k < (4 if d == 0 else 3):
                            send_first(h, d, k + 1)
                        send_own_group(h, f)

            return run

        def step_second(k, b):
            def run():
                for h in range(2):
                    for d in range(2):
                        wait_second(h, d, k, b)
                        if k < 3 or b == d:
                            forward(h, d, k, b)

            return run

        def step_last():
            for h in range(2):
                for d in range(2):
                    wait_second(h, d, 4, d)

        steps = [step_own] + [step_first(k) for k in range(1, 5)]
        steps += [step_second(k, b) for k in range(1, 4) for b in range(2)]
        steps.append(step_last)

        def finish():
            for h in range(2):
                for d in range(2):
                    for slot, ref in (
                        (0, buf.at[0, pl.ds(0, 4 - d), 0]),
                        (1, buf.at[0, :, 0]),
                        (2, buf.at[0, :, 0]),
                        (3, buf.at[0, :, 0]),
                        (4, buf.at[0, pl.ds(0, 4), 0]),
                    ):
                        remote(
                            ref, ref, ssem.at[ps, h, d, slot], rp1.at[ps, h, d, 0], sib
                        ).wait_send()

        return steps, finish

    wsteps, wfinish = gather_steps(0, gv)
    dsteps, dfinish = gather_steps(1, dn)

    order = (2, 1, 3, 0)

    def reducer(own, sendb, recvb, sx, rx, ss, rs, xss, xrs):
        dest = (xm, xp, xp, xp, xm, xm)

        def xcopy(j):
            return remote(sx.at[j], rx.at[j], xss.at[j], xrs.at[j], dest[j])

        def to_sib(i):
            return remote(sendb.at[i], recvb.at[i], ss.at[i], rs.at[i], sib)

        def total(i, half):
            rows = slice(32 * half, 32 * half + 32)
            return own[i, rows].astype(F32) + recvb[i, rows].astype(F32)

        def stage(i):
            to_sib(i).wait_recv()
            if i == 0:
                sx[0] = total(0, 0).astype(BF16)
                xcopy(0).start()
                sx[1] = total(0, 1).astype(BF16)
                xcopy(1).start()
            elif i == 1:
                sx[2] = total(1, 0).astype(BF16)
                xcopy(2).start()
            elif i == 2:
                sx[4] = total(2, 1).astype(BF16)
                xcopy(4).start()

        def relay():
            xcopy(1).wait_recv()
            sx[3] = (total(1, 1) + rx[1].astype(F32)).astype(BF16)
            xcopy(3).start()
            xcopy(0).wait_recv()
            sx[5] = (total(2, 0) + rx[0].astype(F32)).astype(BF16)
            xcopy(5).start()

        def result():
            for j in (2, 4, 3, 5):
                xcopy(j).wait_recv()
            low = total(3, 0) + rx[2].astype(F32) + rx[5].astype(F32)
            high = total(3, 1) + rx[4].astype(F32) + rx[3].astype(F32)
            return low, high

        def finish():
            for i in range(4):
                to_sib(i).wait_send()
            for j in range(6):
                xcopy(j).wait_send()

        return to_sib, stage, relay, result, finish

    def kv_copy():
        return remote(
            kvx.at[:, :, pl.ds(512, 128)],
            kvx.at[:, :, pl.ds(0, 128)],
            kv_sem.at[0],
            kv_sem.at[1],
            nxt,
        )

    kv_copy().start()
    wsteps[0]()
    kv_copy().wait_recv()

    to_sib, stage, relay, result, rfinish = reducer(
        p_own, p_sib, r_sib, s_x, r_x, a_ss, a_rs, ax_ss, ax_rs
    )

    def attend(i):
        n = (x + order[i]) % 4
        row = lax.broadcasted_iota(jnp.int32, (WINDOW, 2 * WINDOW), 0)
        col = lax.broadcasted_iota(jnp.int32, (WINDOW, 2 * WINDOW), 1)
        start = jnp.where((n == 0) & (sp == 0), WINDOW, 0)
        seen = (col > row) & (col <= row + WINDOW) & (col >= start)
        off = pl.multiple_of(n * WINDOW, WINDOW)
        kt = kvx[0, :, pl.ds(off, 2 * WINDOW)]
        vt = kvx[1, :, pl.ds(off, 2 * WINDOW)]
        nil = jnp.zeros_like(kt)
        keys = (jnp.concatenate([kt, nil], axis=0), jnp.concatenate([nil, kt], axis=0))
        vals = (jnp.concatenate([vt, nil], axis=0), jnp.concatenate([nil, vt], axis=0))
        for g in range(2):
            q2 = q_ref[pl.ds(off, WINDOW), 128 * g : 128 * g + 128]
            acc = jnp.zeros((WINDOW, 128), F32)
            for e in range(2):
                sink = sink_ref[2 * g + e]
                scores = jnp.dot(q2, keys[e], preferred_element_type=F32) * HD**-0.5
                scores = jnp.where(seen, scores, NEG_FILL)
                top = jnp.maximum(jnp.max(scores, axis=-1, keepdims=True), sink)
                expo = jnp.exp(scores - top)
                total = jnp.sum(expo, axis=-1, keepdims=True) + jnp.exp(sink - top)
                probs = (expo / total).astype(BF16)
                acc = acc + lax.dot_general(probs, vals[e], NT, preferred_element_type=F32)
            att[:, 128 * g : 128 * g + 128] = acc.astype(BF16)
        for j in range(4):
            cols = slice(512 * j, 512 * j + 512)
            for half, dst in ((1 - c, p_sib), (c, p_own)):
                part = att[pl.ds(pl.multiple_of(64 * half, 64), 64), :]
                dst[i, :, cols] = jnp.dot(
                    part, ow_ref[:, cols], preferred_element_type=F32
                ).astype(BF16)
        to_sib(i).start()

    attend(0)
    wsteps[1]()
    attend(1)
    stage(0)
    wsteps[2]()
    attend(2)
    stage(1)
    wsteps[3]()
    attend(3)
    stage(2)
    wsteps[4]()
    relay()
    stage(3)
    wsteps[5]()

    halves = result()
    for h in range(2):
        rows = slice(32 * h, 32 * h + 32)
        middle = res_ref[rows, :].astype(F32) + rms_scale(halves[h]) * ga_ref[...]
        mid[rows, :] = middle
        x_all[tp, h] = (rms_scale(middle) * gb_ref[...]).astype(BF16)

    tpm, tpp, tp2 = tp_at(x + 3, c), tp_at(x + 1, c), tp_at(x + 2, c)

    def gcopy(j):
        idx, half, dev = (
            (tp, 0, xp), (tp, 1, xm), (tp, 1, xp), (tp, 0, xm), (tpm, 0, xp), (tpp, 1, xm),
            (tpm, 0, sib), (tpp, 1, sib), (tpm, 1, sib), (tpp, 0, sib), (tp2, 0, sib), (tp2, 1, sib),
        )[j]
        ref = x_all.at[idx, half]
        return remote(ref, ref, g_ss.at[j], g_rs.at[j], dev)

    def gown():
        ref = x_all.at[tp]
        return remote(ref, ref, g_ss.at[12], g_rs.at[12], sib)

    for j in range(4):
        gcopy(j).start()
    gown().start()
    wsteps[6]()
    gcopy(0).wait_recv()
    gcopy(4).start()
    gcopy(6).start()
    gcopy(1).wait_recv()
    gcopy(5).start()
    gcopy(7).start()
    wsteps[7]()
    gcopy(2).wait_recv()
    gcopy(8).start()
    gcopy(3).wait_recv()
    gcopy(9).start()
    wsteps[8]()
    dsteps[0]()
    gcopy(4).wait_recv()
    gcopy(10).start()
    gcopy(5).wait_recv()
    gcopy(11).start()
    for j in range(6, 12):
        gcopy(j).wait_recv()
    gown().wait_recv()
    wsteps[9]()
    dsteps[1]()
    wsteps[10]()
    dsteps[2]()
    wsteps[11]()
    dsteps[3]()

    def up_copy(k):
        return remote(
            up.at[k, pl.ds(512, 8), :], up.at[k, pl.ds(0, 8), :], up_ss.at[k], up_rs.at[k], nxt
        )

    def project(k):
        width = 256 if k < 5 else 128
        cols = slice(256 * k, 256 * k + width)
        for m in range(2):
            left = x_all[4 * m : 4 * m + 4].reshape(256, 2048)
            right = gv[:, :, :, :, cols].reshape(2048, width)
            made = jnp.dot(left, right, preferred_element_type=F32)
            up[k, 8 + 256 * m : 264 + 256 * m, 0:width] = made.astype(BF16).astype(F32)
        up_copy(k).start()

    def conv(k, lanes, taps):
        total = taps[0:1] * up[k, 6:518, lanes]
        total = total + taps[1:2] * up[k, 7:519, lanes]
        return total + taps[2:3] * up[k, 8:520, lanes]

    def silu(v):
        return v / (1.0 + jnp.exp(-v))

    def gate(k):
        up_copy(k).wait_recv()
        up[k, 0:8, :] = jnp.where(sp > 0, up[k, 0:8, :], 0.0)
        if k < 5:
            cols = slice(128 * k, 128 * k + 128)
            made = silu(conv(k, slice(0, 128), gt_ref[:, cols])) * conv(
                k, slice(128, 256), vt2_ref[:, cols]
            )
        else:
            cols = slice(640, 768)
            taps = jnp.concatenate([gt_ref[:, 640:704], vt2_ref[:, 640:704]], axis=1)
            both = conv(k, slice(0, 128), taps)
            lane = lax.broadcasted_iota(jnp.int32, both.shape, 1)
            made = jnp.where(lane < 64, silu(both) * pltpu.roll(both, 64, 1), 0.0)
        hid[:, :, cols] = made.astype(BF16).reshape(8, 64, 128)

    project(0)
    project(1)
    dsteps[4]()
    project(2)
    project(3)
    dsteps[5]()
    project(4)
    project(5)
    dsteps[6]()
    gate(0)
    gate(1)
    gate(2)
    dsteps[7]()
    gate(3)
    gate(4)
    gate(5)
    for s in dsteps[8:]:
        s()

    to_sib2, stage2, relay2, result2, rfinish2 = reducer(
        f_own, f_sib, g_sib, t_x, u_x, b_ss, b_rs, bx_ss, bx_rs
    )
    for i in range(4):
        n = (x + order[i]) % 4
        for half, dst in ((1 - c, f_sib), (c, f_own)):
            left = hid[2 * n + half]
            for j in range(4):
                right = dn[2 * j : 2 * j + 2].reshape(512, 768)
                dst[i, :, 512 * j : 512 * j + 512] = lax.dot_general(
                    left, right, NT, preferred_element_type=F32
                ).astype(BF16)
        to_sib2(i).start()
        if i > 0:
            stage2(i - 1)
    relay2()
    stage2(3)
    halves = result2()
    for h in range(2):
        rows = slice(32 * h, 32 * h + 32)
        out_ref[rows, :] = (mid[rows, :] + rms_scale(halves[h]) * gc_ref[...]).astype(BF16)

    kv_copy().wait_send()
    for k in range(6):
        up_copy(k).wait_send()
    for j in range(12):
        gcopy(j).wait_send()
    gown().wait_send()
    rfinish()
    rfinish2()
    wfinish()
    dfinish()


def on_device(
    queries, key_states, value_states, sink_logits, out_weight, residual,
    gain_attn, gain_before, gain_after, gate_weight, value_weight, gate_taps, value_taps, down_weight,
):
    dma = pltpu.SemaphoreType.DMA
    vmem = pl.BlockSpec(memory_space=pltpu.VMEM)
    specs = [vmem] * 14
    specs[3] = pl.BlockSpec(memory_space=pltpu.SMEM)
    reduce_bufs = [
        pltpu.VMEM((4, 64, 2048), BF16),
        pltpu.VMEM((4, 64, 2048), BF16),
        pltpu.VMEM((4, 64, 2048), BF16),
        pltpu.VMEM((6, 32, 2048), BF16),
        pltpu.VMEM((6, 32, 2048), BF16),
    ]
    return pl.pallas_call(
        kernel,
        out_shape=jax.ShapeDtypeStruct((64, 2048), BF16),
        in_specs=specs,
        out_specs=vmem,
        scratch_shapes=[
            pltpu.VMEM((8, 8, 2, 16, 1408), BF16),
            pltpu.VMEM((8, 8, 2, 16, 768), BF16),
            pltpu.VMEM((2, 64, 640), BF16),
            pltpu.VMEM((128, 256), BF16),
            pltpu.VMEM((8, 2, 32, 2048), BF16),
            pltpu.VMEM((6, 520, 256), F32),
            pltpu.VMEM((8, 64, 768), BF16),
            pltpu.VMEM((64, 2048), F32),
            *reduce_bufs,
            *reduce_bufs,
            dma((2, 2, 2, 4)),
            dma((2, 2, 2, 4, 2)),
            dma((2, 2, 2, 5)),
            dma((2,)),
            dma((6,)),
            dma((6,)),
            dma((4,)),
            dma((4,)),
            dma((6,)),
            dma((6,)),
            dma((4,)),
            dma((4,)),
            dma((6,)),
            dma((6,)),
            dma((13,)),
            dma((13,)),
        ],
        compiler_params=pltpu.CompilerParams(
            collective_id=0, has_side_effects=True, vmem_limit_bytes=58 * 1024 * 1024
        ),
    )(
        queries, key_states.T, value_states.T, sink_logits, out_weight, residual,
        gain_attn.reshape(1, -1), gain_before.reshape(1, -1), gain_after.reshape(1, -1),
        gate_weight, value_weight, gate_taps, value_taps, down_weight.T,
    )


def solution(mesh):
    in_specs = (
        P("sp", "tp"), P("sp", "tp"), P("sp", "tp"), P("tp"), P("tp", None), P(("sp", "tp"), None),
        P(), P(), P(), P("sp", "tp"), P("sp", "tp"), P(None, "tp"), P(None, "tp"), P("tp", "sp"),
    )
    return jax.shard_map(
        on_device, mesh=mesh, in_specs=in_specs, out_specs=P(("sp", "tp"), None), check_vma=False
    )
```

time: 239 us -> 99.3 us (0.42)
  waiting for transfers between devices: 126 us -> 0 us
  Pallas kernels: 0 us -> 96.8 us
  blocking collectives: 34.6 us -> 0 us
  starting transfers between devices: 25.4 us -> 0 us
  matrix products: 21 us -> 0 us
  between operations: 13.7 us -> 0.01 us
  other arithmetic: 10.6 us -> 0 us
  local copies, waits for them, and re-layouts: 6.82 us -> 1.67 us
    pallas_call x0 -> x1, Pallas kernels: none -> 96.8 us  [on_device(): pl.pallas_call(kernel, out_shape=jax.ShapeDtypeStruct((64, 2048), BF16),...]
    all_gather x2 -> x0, waiting for transfers between devices: 73 us -> none  [the longest x1 64.6 us: on_device(): down_whole = lax.all_gather(down_weight, 'sp', axis=1, tiled=True)]
    all_to_all x2 -> x0, waiting for transfers between devices: 51.8 us -> none  [the longest x1 26.3 us: sent_to_all(): return lax.all_to_all(copies, axis, split_axis=0, concat_axis=0, tiled=True)]
    all_to_all x1 -> x0, blocking collectives: 34.6 us -> none  [sum_at_owner(): lax.all_to_all(in_blocks(shard, dim, peers), axis, 0, 0, tiled=True)]
    dot_general x6 -> x0, matrix products: 21 us -> none  [the longest x1 9.1 us: on_device(): jnp.dot(selected, down_whole, preferred_element_type=jnp.float32)]
    ppermute x4 -> x0, starting transfers between devices: 13.5 us -> none  [passed_along(): return lax.ppermute(block, axis, route)]
    all_to_all x2 -> x0, starting transfers between devices: 11.8 us -> none  [the longest x1 6.45 us: sum_at_owner(): lax.all_to_all(in_blocks(shard, dim, peers), axis, 0, 0, tiled=True)]
    convert_element_type x4 -> x0, other arithmetic: 4.36 us -> none  [the longest x2 3.24 us: causal_local(): padded = jnp.concatenate([earlier, upward], axis=0).astype(jnp.float32)]
  transfers between devices with their start and end apart: 8 -> 0, of which waited for: 5 -> 0; matrix products, arithmetic and copies ran while one was open for 11% -> 0% of each run, Pallas kernels for 0% -> 0%
where the time goes in v1:
time: 99.3 us; the launch traced here: 98.5 us
  Pallas kernels  96.8 us (97%)
  local copies, waits for them, and re-layouts  1.67 us (2%)
    pallas_call x1, Pallas kernels, on_device(): pl.pallas_call(kernel, out_shape=jax.ShapeDtypeStruct((64, 2048), BF16),...  96.8 us

profile of v1, /device:TPU:1, one launch (start us, length us, event | category | flops | bytes accessed | tf_op | source)
XLA Modules:
  0.0 98.5 jit_solution(5435051262985381235)
XLA Ops:
  0.0 96.8 %shard_map.136 = bf16[64,2048]{1,0:T(8,128)(2,1)} custom-call(bf16[512,256]{1,0:T(8,128)(2,1)} %q_ref.1, bf16[64,512]{1,0:T(8,128)(2,1)} %bitcast.6, bf16[64,512]{1,0:T(8,128)(2,1)} %bitcast.7, f32[4]{0:T(128)} %sink_ref.1, bf16[256,2048]{1,0:T(8,128)(2,1)} %ow_ref.1, bf16[64,2048]{1,0:T(8,128)(2,1)} %res_ref.1, f32[1,2048]{1,0:T(1,128)} %bitcast.9, ...), custom_call_target="tpu_custom_call" | custom-call | tf_op jit(solution)/shard_map/pallas_call | solution.py:456
  96.8 1.7 %copy.16 = bf16[64,2048]{1,0:T(8,128)(2,1)} copy(bf16[64,2048]{1,0:T(8,128)(2,1)} %shard_map.136) | data formatting | bytes 524288

commit v2 on v1

--- a/solution.py
+++ b/solution.py
@@ -24,9 +24,9 @@
     out_ref,
     gv, dn, kvx, att, x_all, up, hid, mid,
     p_own, p_sib, r_sib, s_x, r_x,
-    f_own, f_sib, g_sib, t_x, u_x,
-    rp1, rp2, ssem, kv_sem, up_ss, up_rs,
-    a_ss, a_rs, ax_ss, ax_rs, b_ss, b_rs, bx_ss, bx_rs, g_ss, g_rs,
+    f_own, f_sib, g_sib, t_x, u_x, t_r, u_r, nat, squares,
+    wp1, wp2, w_ss, dp1, dp2, d_ss, kv_sem, up_ss, up_rs,
+    a_ss, a_rs, ax_ss, ax_rs, g_ss, g_rs, b_ss, b_rs,
 ):
     sp = lax.axis_index("sp")
     tp = lax.axis_index("tp")
@@ -72,7 +72,8 @@
 
     pl.semaphore_wait(barrier, 9)
 
-    def gather_steps(ps, buf):
+    def gather_steps(buf, rp1, rp2, ssem, size):
+        count = 8 // size
         first = (y, z)
         second = (z, y)
         fdev = (yn, zn)
@@ -84,78 +85,71 @@
 
         def batch(h, b, s):
             s = s % 8
-            return buf.at[s, pl.ds(4 * b, 4), 0] if h == 0 else buf.at[pl.ds(4 * b, 4), s, 1]
+            part = pl.ds(size * b, size)
+            return buf.at[s, part, 0] if h == 0 else buf.at[part, s, 1]
+
+        def hop(h, d, k):
+            return first[h] + 8 - k if d == 0 else first[h] + k
+
+        def group(h, d, k):
+            return second[h] + 8 - k if d == 0 else second[h] + k
 
         def send_first(h, d, k):
-            f, s = first[h], second[h]
-            ref = item(h, f + 9 - k if d == 0 else f + k - 1, s)
-            remote(ref, ref, ssem.at[ps, h, d, 0], rp1.at[ps, h, d, k - 1], fdev[h][d]).start()
+            ref = item(h, hop(h, d, k - 1), second[h])
+            remote(ref, ref, ssem.at[h, d, 0], rp1.at[h, d, k - 1], fdev[h][d]).start()
 
         def wait_first(h, d, k):
-            f, s = first[h], second[h]
-            ref = item(h, f + 8 - k if d == 0 else f + k, s)
-            remote(ref, ref, ssem.at[ps, h, d, 0], rp1.at[ps, h, d, k - 1], fdev[h][d]).wait_recv()
-            return f + 8 - k if d == 0 else f + k
-
-        def send_own_group(h, f):
+            ref = item(h, hop(h, d, k), second[h])
+            remote(ref, ref, ssem.at[h, d, 0], rp1.at[h, d, k - 1], fdev[h][d]).wait_recv()
+
+        def send_item(h, f):
             f = f % 8
             ref = item(h, f, second[h])
             for d in range(2):
-                remote(
-                    ref, ref, ssem.at[ps, h, d, 1], rp2.at[ps, h, d, 0, f // 4], sdev[h][d]
-                ).start()
-
-        def group(h, d, k):
-            return second[h] + 8 - k if d == 0 else second[h] + k
+                remote(ref, ref, ssem.at[h, d, 1], rp2.at[h, d, 0, f // size], sdev[h][d]).start()
 
         def wait_second(h, d, k, b):
             ref = batch(h, b, group(h, d, k))
-            remote(
-                ref, ref, ssem.at[ps, h, d, 1], rp2.at[ps, h, d, k - 1, b], sdev[h][d]
-            ).wait_recv()
+            remote(ref, ref, ssem.at[h, d, 1], rp2.at[h, d, k - 1, b], sdev[h][d]).wait_recv()
 
         def forward(h, d, k, b):
             ref = batch(h, b, group(h, d, k))
-            remote(
-                ref, ref, ssem.at[ps, h, d, k + 1], rp2.at[ps, h, d, k, b], sdev[h][d]
-            ).start()
-
-        def step_own():
+            remote(ref, ref, ssem.at[h, d, k + 1], rp2.at[h, d, k, b], sdev[h][d]).start()
+
+        def step_own(items):
             for h in range(2):
                 for d in range(2):
                     send_first(h, d, 1)
-            for h in range(2):
-                send_own_group(h, first[h])
-
-        def step_first(k):
-            def run():
-                for d in range(2 if k < 4 else 1):
-                    for h in range(2):
-                        f = wait_first(h, d, k)
-                        if k < (4 if d == 0 else 3):
-                            send_first(h, d, k + 1)
-                        send_own_group(h, f)
-
-            return run
-
-        def step_second(k, b):
-            def run():
+            if items:
+                for h in range(2):
+                    send_item(h, first[h])
+
+        def step_first(k, items):
+            for d in range(2 if k < 4 else 1):
+                for h in range(2):
+                    wait_first(h, d, k)
+                    if k < 4 - d:
+                        send_first(h, d, k + 1)
+                    if items:
+                        send_item(h, hop(h, d, k))
+
+        def step_group():
+            for b in range(count):
                 for h in range(2):
                     for d in range(2):
-                        wait_second(h, d, k, b)
-                        if k < 3 or b == d:
-                            forward(h, d, k, b)
-
-            return run
-
-        def step_last():
+                        forward(h, d, 0, b)
+
+        def step_second(k, b):
             for h in range(2):
                 for d in range(2):
-                    wait_second(h, d, 4, d)
-
-        steps = [step_own] + [step_first(k) for k in range(1, 5)]
-        steps += [step_second(k, b) for k in range(1, 4) for b in range(2)]
-        steps.append(step_last)
+                    wait_second(h, d, k, b)
+                    if k < 3 or b // (count // 2) == d:
+                        forward(h, d, k, b)
+
+        def step_last(b):
+            for h in range(2):
+                for d in range(2):
+                    wait_second(h, d, 4, d * (count // 2) + b)
 
         def finish():
             for h in range(2):
@@ -167,14 +161,12 @@
                         (3, buf.at[0, :, 0]),
                         (4, buf.at[0, pl.ds(0, 4), 0]),
                     ):
-                        remote(
-                            ref, ref, ssem.at[ps, h, d, slot], rp1.at[ps, h, d, 0], sib
-                        ).wait_send()
-
-        return steps, finish
-
-    wsteps, wfinish = gather_steps(0, gv)
-    dsteps, dfinish = gather_steps(1, dn)
+                        remote(ref, ref, ssem.at[h, d, slot], rp1.at[h, d, 0], sib).wait_send()
+
+        return step_own, step_first, step_group, step_second, step_last, finish
+
+    w_own, w_first, _, w_second, w_last, w_finish = gather_steps(gv, wp1, wp2, w_ss, 4)
+    d_own, d_first, d_group, d_second, d_last, d_finish = gather_steps(dn, dp1, dp2, d_ss, 2)
 
     order = (2, 1, 3, 0)
 
@@ -236,10 +228,6 @@
             kv_sem.at[1],
             nxt,
         )
-
-    kv_copy().start()
-    wsteps[0]()
-    kv_copy().wait_recv()
 
     to_sib, stage, relay, result, rfinish = reducer(
         p_own, p_sib, r_sib, s_x, r_x, a_ss, a_rs, ax_ss, ax_rs
@@ -279,27 +267,16 @@
                 ).astype(BF16)
         to_sib(i).start()
 
-    attend(0)
-    wsteps[1]()
-    attend(1)
-    stage(0)
-    wsteps[2]()
-    attend(2)
-    stage(1)
-    wsteps[3]()
-    attend(3)
-    stage(2)
-    wsteps[4]()
-    relay()
-    stage(3)
-    wsteps[5]()
-
-    halves = result()
-    for h in range(2):
-        rows = slice(32 * h, 32 * h + 32)
-        middle = res_ref[rows, :].astype(F32) + rms_scale(halves[h]) * ga_ref[...]
-        mid[rows, :] = middle
-        x_all[tp, h] = (rms_scale(middle) * gb_ref[...]).astype(BF16)
+    def norms():
+        halves = result()
+        for h in range(2):
+            rows = slice(32 * h, 32 * h + 32)
+            middle = res_ref[rows, :].astype(F32) + rms_scale(halves[h]) * ga_ref[...]
+            mid[rows, :] = middle
+            x_all[tp, h] = (rms_scale(middle) * gb_ref[...]).astype(BF16)
+        for j in range(4):
+            gcopy(j).start()
+        gown().start()
 
     tpm, tpp, tp2 = tp_at(x + 3, c), tp_at(x + 1, c), tp_at(x + 2, c)
 
@@ -315,36 +292,15 @@
         ref = x_all.at[tp]
         return remote(ref, ref, g_ss.at[12], g_rs.at[12], sib)
 
-    for j in range(4):
-        gcopy(j).start()
-    gown().start()
-    wsteps[6]()
-    gcopy(0).wait_recv()
-    gcopy(4).start()
-    gcopy(6).start()
-    gcopy(1).wait_recv()
-    gcopy(5).start()
-    gcopy(7).start()
-    wsteps[7]()
-    gcopy(2).wait_recv()
-    gcopy(8).start()
-    gcopy(3).wait_recv()
-    gcopy(9).start()
-    wsteps[8]()
-    dsteps[0]()
-    gcopy(4).wait_recv()
-    gcopy(10).start()
-    gcopy(5).wait_recv()
-    gcopy(11).start()
-    for j in range(6, 12):
+    def pass_on(j, *after):
         gcopy(j).wait_recv()
-    gown().wait_recv()
-    wsteps[9]()
-    dsteps[1]()
-    wsteps[10]()
-    dsteps[2]()
-    wsteps[11]()
-    dsteps[3]()
+        for k in after:
+            gcopy(k).start()
+
+    def rows_in():
+        for j in range(6, 12):
+            gcopy(j).wait_recv()
+        gown().wait_recv()
 
     def up_copy(k):
         return remote(
@@ -383,48 +339,178 @@
             both = conv(k, slice(0, 128), taps)
             lane = lax.broadcasted_iota(jnp.int32, both.shape, 1)
             made = jnp.where(lane < 64, silu(both) * pltpu.roll(both, 64, 1), 0.0)
-        hid[:, :, cols] = made.astype(BF16).reshape(8, 64, 128)
-
-    project(0)
-    project(1)
-    dsteps[4]()
-    project(2)
-    project(3)
-    dsteps[5]()
-    project(4)
-    project(5)
-    dsteps[6]()
-    gate(0)
-    gate(1)
-    gate(2)
-    dsteps[7]()
-    gate(3)
-    gate(4)
-    gate(5)
-    for s in dsteps[8:]:
-        s()
-
-    to_sib2, stage2, relay2, result2, rfinish2 = reducer(
-        f_own, f_sib, g_sib, t_x, u_x, b_ss, b_rs, bx_ss, bx_rs
-    )
+        made = made.astype(BF16)
+        for b in range(8):
+            slot = (b // 2 + 4 - x) % 4 + 4 * (1 - (c + b) % 2)
+            hid[slot, :, cols] = made[64 * b : 64 * b + 64]
+
+    def groups(k):
+        if k in (0, 4):
+            return [(0, z + k), (1, y + k)]
+        return [(0, z + 8 - k), (0, z + k), (1, y + 8 - k), (1, y + k)]
+
+    edges = (0, 256, 768, 1280, 1792, 2048)
+
+    def span(k):
+        return pl.ds(edges[k], edges[k + 1] - edges[k])
+
+    def sib_copy(k):
+        return remote(
+            f_sib.at[:, :, span(k)], g_sib.at[:, :, span(k)], b_ss.at[0, k], b_rs.at[0, k], sib
+        )
+
+    def x_copy(k, d):
+        return remote(
+            t_x.at[d, :, :, span(k)], u_x.at[d, :, :, span(k)],
+            b_ss.at[1 + d, k], b_rs.at[1 + d, k], (xp, xm)[d],
+        )
+
+    def r_copy(k, d):
+        return remote(
+            t_r.at[d, :, span(k)], u_r.at[d, :, span(k)],
+            b_ss.at[3 + d, k], b_rs.at[3 + d, k], (xp, xm)[d],
+        )
+
+    def down(k):
+        right = [
+            (dn[g % 8, :, 0] if h == 0 else dn[:, g % 8, 1]).reshape(128, 768)
+            for h, g in groups(k)
+        ]
+        made = lax.dot_general(
+            hid[...].reshape(512, 768), jnp.concatenate(right, axis=0), NT,
+            preferred_element_type=F32,
+        ).astype(BF16).reshape(8, 64, 128 * len(right))
+        f_sib[:, :, span(k)] = made[0:4]
+        f_own[:, :, span(k)] = made[4:8]
+        sib_copy(k).start()
+
+    def both(k, i, half):
+        rows = slice(32 * half, 32 * half + 32)
+        return f_own[i, rows, span(k)].astype(F32) + g_sib[i, rows, span(k)].astype(F32)
+
+    def spread(k):
+        sib_copy(k).wait_recv()
+        t_x[0, 0, :, span(k)] = both(k, 2, 1).astype(BF16)
+        t_x[0, 1, :, span(k)] = both(k, 1, 0).astype(BF16)
+        x_copy(k, 0).start()
+        t_x[1, 0, :, span(k)] = both(k, 2, 0).astype(BF16)
+        t_x[1, 1, :, span(k)] = both(k, 3, 1).astype(BF16)
+        x_copy(k, 1).start()
+
+    def relayed(k):
+        x_copy(k, 0).wait_recv()
+        t_r[0, :, span(k)] = (both(k, 1, 1) + u_x[0, 0, :, span(k)].astype(F32)).astype(BF16)
+        r_copy(k, 0).start()
+        x_copy(k, 1).wait_recv()
+        t_r[1, :, span(k)] = (both(k, 3, 0) + u_x[1, 0, :, span(k)].astype(F32)).astype(BF16)
+        r_copy(k, 1).start()
+
+    def place(k):
+        lane = lax.broadcasted_iota(jnp.int32, (32, 128), 1) // 16
+        for half in range(2):
+            rows = slice(32 * half, 32 * half + 32)
+            r_copy(k, 1 - half).wait_recv()
+            total = both(k, 0, half) + u_x[half, 1, :, span(k)].astype(F32)
+            total = total + u_r[1 - half, :, span(k)].astype(F32)
+            for j, (h, g) in enumerate(groups(k)):
+                g = g % 8
+                piece = total[:, 128 * j : 128 * j + 128]
+                if k == 0 and j == 0:
+                    squares[rows, :] = piece * piece
+                else:
+                    squares[rows, :] += piece * piece
+                for t in range(8):
+                    if h == 0:
+                        where, shift, spot = (g, t // 4), 16 * t, 2 * (t % 4)
+                    else:
+                        where, spot = (t, g // 4), 2 * (g % 4) + 1
+                        shift = (16 * spot + 128 - 16 * t) % 128
+                    moved = pltpu.roll(piece, shift, 1)
+                    nat[where[0], where[1], rows, :] = jnp.where(
+                        lane == spot, moved, nat[where[0], where[1], rows, :]
+                    )
+
+    def last():
+        scale = lax.rsqrt(jnp.sum(squares[...], axis=-1, keepdims=True) * (1.0 / 2048) + 1e-06)
+        for j in range(16):
+            cols = slice(128 * j, 128 * j + 128)
+            out_ref[:, cols] = (
+                mid[:, cols] + nat[j // 2, j % 2] * scale * gc_ref[:, cols]
+            ).astype(BF16)
+
+    def run(name, step, *args):
+        with jax.named_scope(name):
+            step(*args)
+
+    run("kv_start", lambda: kv_copy().start())
+    run("w0", w_own, True)
+    run("kv_wait", lambda: kv_copy().wait_recv())
     for i in range(4):
-        n = (x + order[i]) % 4
-        for half, dst in ((1 - c, f_sib), (c, f_own)):
-            left = hid[2 * n + half]
-            for j in range(4):
-                right = dn[2 * j : 2 * j + 2].reshape(512, 768)
-                dst[i, :, 512 * j : 512 * j + 512] = lax.dot_general(
-                    left, right, NT, preferred_element_type=F32
-                ).astype(BF16)
-        to_sib2(i).start()
+        run(f"attend{i}", attend, i)
         if i > 0:
-            stage2(i - 1)
-    relay2()
-    stage2(3)
-    halves = result2()
-    for h in range(2):
-        rows = slice(32 * h, 32 * h + 32)
-        out_ref[rows, :] = (mid[rows, :] + rms_scale(halves[h]) * gc_ref[...]).astype(BF16)
+            run(f"stage{i - 1}", stage, i - 1)
+        run(f"w{i + 1}", w_first, i + 1, True)
+    run("relay", relay)
+    run("stage3", stage, 3)
+    run("w5", w_second, 1, 0)
+    run("d_own", d_own, False)
+    run("norms", norms)
+    run("w6", w_second, 1, 1)
+    run("d_f1", d_first, 1, False)
+    run("pass0", pass_on, 0, 4, 6)
+    run("pass1", pass_on, 1, 5, 7)
+    run("w7", w_second, 2, 0)
+    run("d_f2", d_first, 2, False)
+    run("pass2", pass_on, 2, 8)
+    run("pass3", pass_on, 3, 9)
+    run("w8", w_second, 2, 1)
+    run("d_f3", d_first, 3, False)
+    run("pass4", pass_on, 4, 10)
+    run("pass5", pass_on, 5, 11)
+    run("rows_in", rows_in)
+    run("w9", w_second, 3, 0)
+    run("d_f4", d_first, 4, False)
+    run("w10", w_second, 3, 1)
+    run("d_group", d_group)
+    run("w11", w_last, 0)
+    steps = [(d_second, k, b) for k in range(1, 4) for b in range(4)] + [(d_last, 0), (d_last, 1)]
+
+    def e(j):
+        run(f"e{j}", *steps[j])
+
+    for k in range(6):
+        run(f"project{k}", project, k)
+        e(k)
+    for k in range(6):
+        run(f"gate{k}", gate, k)
+        if k % 2:
+            e(6 + k // 2)
+    run("down0", down, 0)
+    e(9)
+    run("down1", down, 1)
+    run("spread0", spread, 0)
+    e(10)
+    run("down2", down, 2)
+    run("spread1", spread, 1)
+    run("relayed0", relayed, 0)
+    e(11)
+    run("down3", down, 3)
+    run("spread2", spread, 2)
+    run("relayed1", relayed, 1)
+    run("place0", place, 0)
+    e(12)
+    run("spread3", spread, 3)
+    run("relayed2", relayed, 2)
+    run("place1", place, 1)
+    e(13)
+    run("down4", down, 4)
+    run("relayed3", relayed, 3)
+    run("spread4", spread, 4)
+    run("place2", place, 2)
+    run("relayed4", relayed, 4)
+    run("place3", place, 3)
+    run("place4", place, 4)
+    run("last", last)
 
     kv_copy().wait_send()
     for k in range(6):
@@ -433,9 +519,13 @@
         gcopy(j).wait_send()
     gown().wait_send()
     rfinish()
-    rfinish2()
-    wfinish()
-    dfinish()
+    for k in range(5):
+        sib_copy(k).wait_send()
+        for d in range(2):
+            x_copy(k, d).wait_send()
+            r_copy(k, d).wait_send()
+    w_finish()
+    d_finish()
 
 
 def on_device(
@@ -468,15 +558,20 @@
             pltpu.VMEM((8, 64, 768), BF16),
             pltpu.VMEM((64, 2048), F32),
             *reduce_bufs,
-            *reduce_bufs,
-            dma((2, 2, 2, 4)),
-            dma((2, 2, 2, 4, 2)),
-            dma((2, 2, 2, 5)),
+            *reduce_bufs[:3],
+            pltpu.VMEM((2, 2, 32, 2048), BF16),
+            pltpu.VMEM((2, 2, 32, 2048), BF16),
+            pltpu.VMEM((2, 32, 2048), BF16),
+            pltpu.VMEM((2, 32, 2048), BF16),
+            pltpu.VMEM((8, 2, 64, 128), F32),
+            pltpu.VMEM((64, 128), F32),
+            dma((2, 2, 4)),
+            dma((2, 2, 4, 2)),
+            dma((2, 2, 5)),
+            dma((2, 2, 4)),
+            dma((2, 2, 4, 4)),
+            dma((2, 2, 5)),
             dma((2,)),
-            dma((6,)),
-            dma((6,)),
-            dma((4,)),
-            dma((4,)),
             dma((6,)),
             dma((6,)),
             dma((4,)),
@@ -485,6 +580,8 @@
             dma((6,)),
             dma((13,)),
             dma((13,)),
+            dma((5, 5)),
+            dma((5, 5)),
         ],
         compiler_params=pltpu.CompilerParams(
             collective_id=0, has_side_effects=True, vmem_limit_bytes=58 * 1024 * 1024

time: 99.3 us -> 94 us (0.947)
  Pallas kernels: 96.8 us -> 91.3 us
    pallas_call x1, Pallas kernels: 96.8 us -> 91.3 us  [on_device(): pl.pallas_call(kernel, out_shape=jax.ShapeDtypeStruct((64, 2048), BF16),...]
where the time goes in v2:
time: 94 us; the launch traced here: 92.9 us
  Pallas kernels  91.3 us (97%)
  local copies, waits for them, and re-layouts  1.67 us (2%)
    pallas_call x1, Pallas kernels, on_device(): pl.pallas_call(kernel, out_shape=jax.ShapeDtypeStruct((64, 2048), BF16),...  91.3 us

profile of v2, /device:TPU:1, one launch (start us, length us, event | category | flops | bytes accessed | tf_op | source)
XLA Modules:
  0.0 92.9 jit_solution(18066406993502814837)
XLA Ops:
  0.0 91.3 %shard_map.136 = bf16[64,2048]{1,0:T(8,128)(2,1)} custom-call(bf16[512,256]{1,0:T(8,128)(2,1)} %q_ref.1, bf16[64,512]{1,0:T(8,128)(2,1)} %bitcast.6, bf16[64,512]{1,0:T(8,128)(2,1)} %bitcast.7, f32[4]{0:T(128)} %sink_ref.1, bf16[256,2048]{1,0:T(8,128)(2,1)} %ow_ref.1, bf16[64,2048]{1,0:T(8,128)(2,1)} %res_ref.1, f32[1,2048]{1,0:T(1,128)} %bitcast.9, ...), custom_call_target="tpu_custom_call" | custom-call | tf_op jit(solution)/shard_map/pallas_call | solution.py:546
  91.3 1.7 %copy.16 = bf16[64,2048]{1,0:T(8,128)(2,1)} copy(bf16[64,2048]{1,0:T(8,128)(2,1)} %shard_map.136) | data formatting | bytes 524288

commit v3 on v2

--- a/solution.py
+++ b/solution.py
@@ -19,9 +19,10 @@
 
 
 def kernel(
-    q_ref, kt_ref, vt_ref, sink_ref, ow_ref, res_ref, ga_ref, gb_ref, gc_ref,
-    gw_ref, vw_ref, gt_ref, vt2_ref, dw_ref,
+    q_hbm, kt_hbm, vt_hbm, sink_ref, ow_hbm, res_hbm, ga_ref, gb_ref, gc_ref,
+    gw_hbm, vw_hbm, gt_ref, vt2_ref, dw_hbm,
     out_ref,
+    q_ref, ow_ref, res_ref, gw_ref, vw_ref, dw_ref, in_sem,
     gv, dn, kvx, att, x_all, up, hid, mid,
     p_own, p_sib, r_sib, s_x, r_x,
     f_own, f_sib, g_sib, t_x, u_x, t_r, u_r, nat, squares,
@@ -49,11 +50,27 @@
     for dev in (nxt, prv, sib, xp, xm, *zn, *yn):
         pl.semaphore_signal(barrier, inc=1, device_id=dev, device_id_type=MESH)
 
+    loads = (
+        (q_hbm, q_ref), (ow_hbm, ow_ref), (res_hbm, res_ref), (gw_hbm, gw_ref), (vw_hbm, vw_ref),
+        (dw_hbm, dw_ref), (kt_hbm, kvx.at[0, :, pl.ds(128, 512)]), (vt_hbm, kvx.at[1, :, pl.ds(128, 512)]),
+    )
+
+    def load(j):
+        return pltpu.make_async_copy(loads[j][0], loads[j][1], in_sem.at[j])
+
+    def fetched(*which):
+        for j in which:
+            load(j).wait()
+
+    for j in (3, 4, 5, 6, 7, 0, 1, 2):
+        load(j).start()
+
     def remote(src, dst, ss, rs, dev):
         return pltpu.make_async_remote_copy(
             src_ref=src, dst_ref=dst, send_sem=ss, recv_sem=rs, device_id=dev, device_id_type=MESH
         )
 
+    fetched(3, 4, 5, 6, 7)
     for h in range(2):
         rows = slice(16 * h, 16 * h + 16)
         for k in range(5):
@@ -67,9 +84,6 @@
         dn[z, y, h, :, 640:768] = jnp.concatenate(
             [dw_ref[rows, 640:704].astype(F32), jnp.zeros((16, 64), F32)], axis=1
         ).astype(BF16)
-    kvx[0, :, 128:640] = kt_ref[...]
-    kvx[1, :, 128:640] = vt_ref[...]
-
     pl.semaphore_wait(barrier, 9)
 
     def gather_steps(buf, rp1, rp2, ssem, size):
@@ -78,6 +92,7 @@
         second = (z, y)
         fdev = (yn, zn)
         sdev = (zn, yn)
+        links = tuple((h, d) for h in range(2) for d in range(2))
 
         def item(h, f, s):
             f, s = f % 8, s % 8
@@ -85,7 +100,7 @@
 
         def batch(h, b, s):
             s = s % 8
-            part = pl.ds(size * b, size)
+            part = pl.ds(size * ((first[h] // size + b) % count), size)
             return buf.at[s, part, 0] if h == 0 else buf.at[part, s, 1]
 
         def hop(h, d, k):
@@ -94,78 +109,65 @@
         def group(h, d, k):
             return second[h] + 8 - k if d == 0 else second[h] + k
 
+        def arrived(items, sem):
+            ref = buf.at[0, pl.ds(0, items), 0]
+            remote(ref, ref, ssem.at[0], sem, sib).wait_recv()
+
         def send_first(h, d, k):
             ref = item(h, hop(h, d, k - 1), second[h])
-            remote(ref, ref, ssem.at[h, d, 0], rp1.at[h, d, k - 1], fdev[h][d]).start()
-
-        def wait_first(h, d, k):
-            ref = item(h, hop(h, d, k), second[h])
-            remote(ref, ref, ssem.at[h, d, 0], rp1.at[h, d, k - 1], fdev[h][d]).wait_recv()
+            remote(ref, ref, ssem.at[0], rp1.at[k - 1], fdev[h][d]).start()
 
         def send_item(h, f):
             f = f % 8
             ref = item(h, f, second[h])
+            slot = (f // size + count - first[h] // size) % count
             for d in range(2):
-                remote(ref, ref, ssem.at[h, d, 1], rp2.at[h, d, 0, f // size], sdev[h][d]).start()
-
-        def wait_second(h, d, k, b):
-            ref = batch(h, b, group(h, d, k))
-            remote(ref, ref, ssem.at[h, d, 1], rp2.at[h, d, k - 1, b], sdev[h][d]).wait_recv()
+                remote(ref, ref, ssem.at[1], rp2.at[0, slot], sdev[h][d]).start()
 
         def forward(h, d, k, b):
             ref = batch(h, b, group(h, d, k))
-            remote(ref, ref, ssem.at[h, d, k + 1], rp2.at[h, d, k, b], sdev[h][d]).start()
+            slot = b if k < 3 else b // 2
+            remote(ref, ref, ssem.at[1], rp2.at[k, slot], sdev[h][d]).start()
 
         def step_own(items):
-            for h in range(2):
-                for d in range(2):
-                    send_first(h, d, 1)
+            for h, d in links:
+                send_first(h, d, 1)
             if items:
                 for h in range(2):
                     send_item(h, first[h])
 
         def step_first(k, items):
-            for d in range(2 if k < 4 else 1):
-                for h in range(2):
-                    wait_first(h, d, k)
-                    if k < 4 - d:
-                        send_first(h, d, k + 1)
-                    if items:
+            arrived(4 if k < 4 else 2, rp1.at[k - 1])
+            for h, d in links:
+                if k < 4 - d:
+                    send_first(h, d, k + 1)
+            if items:
+                for h, d in links:
+                    if k <= 4 - d:
                         send_item(h, hop(h, d, k))
 
-        def step_group():
-            for b in range(count):
-                for h in range(2):
-                    for d in range(2):
-                        forward(h, d, 0, b)
+        def step_group(b):
+            for h, d in links:
+                forward(h, d, 0, b)
 
         def step_second(k, b):
-            for h in range(2):
-                for d in range(2):
-                    wait_second(h, d, k, b)
-                    if k < 3 or b // (count // 2) == d:
-                        forward(h, d, k, b)
+            arrived(4 * size, rp2.at[k - 1, b])
+            for h, d in links:
+                if k < 3 or (b in (1, 2)) == d:
+                    forward(h, d, k, b)
 
         def step_last(b):
-            for h in range(2):
-                for d in range(2):
-                    wait_second(h, d, 4, d * (count // 2) + b)
+            arrived(4 * size, rp2.at[3, b])
 
         def finish():
-            for h in range(2):
-                for d in range(2):
-                    for slot, ref in (
-                        (0, buf.at[0, pl.ds(0, 4 - d), 0]),
-                        (1, buf.at[0, :, 0]),
-                        (2, buf.at[0, :, 0]),
-                        (3, buf.at[0, :, 0]),
-                        (4, buf.at[0, pl.ds(0, 4), 0]),
-                    ):
-                        remote(ref, ref, ssem.at[h, d, slot], rp1.at[h, d, 0], sib).wait_send()
+            ref = buf.at[0, pl.ds(0, 7)]
+            remote(ref, ref, ssem.at[0], rp1.at[0], sib).wait_send()
+            ref = buf.at[pl.ds(0, 7)]
+            remote(ref, ref, ssem.at[1], rp1.at[0], sib).wait_send()
 
         return step_own, step_first, step_group, step_second, step_last, finish
 
-    w_own, w_first, _, w_second, w_last, w_finish = gather_steps(gv, wp1, wp2, w_ss, 4)
+    w_own, w_first, _, w_second, w_last, w_finish = gather_steps(gv, wp1, wp2, w_ss, 2)
     d_own, d_first, d_group, d_second, d_last, d_finish = gather_steps(dn, dp1, dp2, d_ss, 2)
 
     order = (2, 1, 3, 0)
@@ -174,10 +176,10 @@
         dest = (xm, xp, xp, xp, xm, xm)
 
         def xcopy(j):
-            return remote(sx.at[j], rx.at[j], xss.at[j], xrs.at[j], dest[j])
+            return remote(sx.at[j], rx.at[j], xss.at[0], xrs.at[min(j, 2)], dest[j])
 
         def to_sib(i):
-            return remote(sendb.at[i], recvb.at[i], ss.at[i], rs.at[i], sib)
+            return remote(sendb.at[i], recvb.at[i], ss.at[0], rs.at[i], sib)
 
         def total(i, half):
             rows = slice(32 * half, 32 * half + 32)
@@ -206,17 +208,15 @@
             xcopy(5).start()
 
         def result():
-            for j in (2, 4, 3, 5):
-                xcopy(j).wait_recv()
+            ref = rx.at[pl.ds(2, 4)]
+            remote(ref, ref, xss.at[0], xrs.at[2], xp).wait_recv()
             low = total(3, 0) + rx[2].astype(F32) + rx[5].astype(F32)
             high = total(3, 1) + rx[4].astype(F32) + rx[3].astype(F32)
             return low, high
 
         def finish():
-            for i in range(4):
-                to_sib(i).wait_send()
-            for j in range(6):
-                xcopy(j).wait_send()
+            remote(sendb, recvb, ss.at[0], rs.at[0], sib).wait_send()
+            remote(sx, rx, xss.at[0], xrs.at[0], xp).wait_send()
 
         return to_sib, stage, relay, result, finish
 
@@ -286,11 +286,11 @@
             (tpm, 0, sib), (tpp, 1, sib), (tpm, 1, sib), (tpp, 0, sib), (tp2, 0, sib), (tp2, 1, sib),
         )[j]
         ref = x_all.at[idx, half]
-        return remote(ref, ref, g_ss.at[j], g_rs.at[j], dev)
+        return remote(ref, ref, g_ss.at[0], g_rs.at[min(j, 6)], dev)
 
     def gown():
         ref = x_all.at[tp]
-        return remote(ref, ref, g_ss.at[12], g_rs.at[12], sib)
+        return remote(ref, ref, g_ss.at[0], g_rs.at[6], sib)
 
     def pass_on(j, *after):
         gcopy(j).wait_recv()
@@ -298,13 +298,12 @@
             gcopy(k).start()
 
     def rows_in():
-        for j in range(6, 12):
-            gcopy(j).wait_recv()
-        gown().wait_recv()
+        ref = x_all.at[pl.ds(0, 4)]
+        remote(ref, ref, g_ss.at[0], g_rs.at[6], sib).wait_recv()
 
     def up_copy(k):
         return remote(
-            up.at[k, pl.ds(512, 8), :], up.at[k, pl.ds(0, 8), :], up_ss.at[k], up_rs.at[k], nxt
+            up.at[k, pl.ds(512, 8), :], up.at[k, pl.ds(0, 8), :], up_ss.at[0], up_rs.at[k], nxt
         )
 
     def project(k):
@@ -345,30 +344,31 @@
             hid[slot, :, cols] = made[64 * b : 64 * b + 64]
 
     def groups(k):
-        if k in (0, 4):
-            return [(0, z + k), (1, y + k)]
-        return [(0, z + 8 - k), (0, z + k), (1, y + 8 - k), (1, y + k)]
-
-    edges = (0, 256, 768, 1280, 1792, 2048)
+        if k == 3:
+            return [(0, z + 4), (1, y + 4)]
+        near = [(0, z + 7 - k), (0, z + k + 1), (1, y + 7 - k), (1, y + k + 1)]
+        return near if k else [(0, z), (1, y)] + near
+
+    edges = (0, 768, 1280, 1792, 2048)
 
     def span(k):
         return pl.ds(edges[k], edges[k + 1] - edges[k])
 
     def sib_copy(k):
         return remote(
-            f_sib.at[:, :, span(k)], g_sib.at[:, :, span(k)], b_ss.at[0, k], b_rs.at[0, k], sib
+            f_sib.at[:, :, span(k)], g_sib.at[:, :, span(k)], b_ss.at[0], b_rs.at[0, k], sib
         )
 
     def x_copy(k, d):
         return remote(
             t_x.at[d, :, :, span(k)], u_x.at[d, :, :, span(k)],
-            b_ss.at[1 + d, k], b_rs.at[1 + d, k], (xp, xm)[d],
+            b_ss.at[1], b_rs.at[1, k], (xp, xm)[d],
         )
 
     def r_copy(k, d):
         return remote(
             t_r.at[d, :, span(k)], u_r.at[d, :, span(k)],
-            b_ss.at[3 + d, k], b_rs.at[3 + d, k], (xp, xm)[d],
+            b_ss.at[2], b_rs.at[2, k], (xp, xm)[d],
         )
 
     def down(k):
@@ -398,18 +398,19 @@
         x_copy(k, 1).start()
 
     def relayed(k):
-        x_copy(k, 0).wait_recv()
+        ref = u_x.at[:, :, :, span(k)]
+        remote(ref, ref, b_ss.at[1], b_rs.at[1, k], xp).wait_recv()
         t_r[0, :, span(k)] = (both(k, 1, 1) + u_x[0, 0, :, span(k)].astype(F32)).astype(BF16)
         r_copy(k, 0).start()
-        x_copy(k, 1).wait_recv()
         t_r[1, :, span(k)] = (both(k, 3, 0) + u_x[1, 0, :, span(k)].astype(F32)).astype(BF16)
         r_copy(k, 1).start()
 
     def place(k):
         lane = lax.broadcasted_iota(jnp.int32, (32, 128), 1) // 16
+        ref = u_r.at[:, :, span(k)]
+        remote(ref, ref, b_ss.at[2], b_rs.at[2, k], xp).wait_recv()
         for half in range(2):
             rows = slice(32 * half, 32 * half + 32)
-            r_copy(k, 1 - half).wait_recv()
             total = both(k, 0, half) + u_x[half, 1, :, span(k)].astype(F32)
             total = total + u_r[1 - half, :, span(k)].astype(F32)
             for j, (h, g) in enumerate(groups(k)):
@@ -444,88 +445,81 @@
 
     run("kv_start", lambda: kv_copy().start())
     run("w0", w_own, True)
+    run("d0", d_own, False)
     run("kv_wait", lambda: kv_copy().wait_recv())
-    for i in range(4):
-        run(f"attend{i}", attend, i)
-        if i > 0:
-            run(f"stage{i - 1}", stage, i - 1)
-        run(f"w{i + 1}", w_first, i + 1, True)
+    run("in_wait", lambda: fetched(0, 1))
+    def first(k):
+        run(f"w{k}", w_first, k, True)
+        run(f"d{k}", d_first, k, False)
+
+    run("attend0", attend, 0)
+    first(1)
+    run("attend1", attend, 1)
+    run("stage0", stage, 0)
+    run("attend2", attend, 2)
+    first(2)
+    run("stage1", stage, 1)
+    run("w1_0", w_second, 1, 0)
+    run("attend3", attend, 3)
+    run("stage2", stage, 2)
+    first(3)
     run("relay", relay)
     run("stage3", stage, 3)
-    run("w5", w_second, 1, 0)
-    run("d_own", d_own, False)
+    first(4)
+    for b in (1, 3, 2):
+        run(f"w1_{b}", w_second, 1, b)
+    run("in_wait2", lambda: fetched(2))
     run("norms", norms)
-    run("w6", w_second, 1, 1)
-    run("d_f1", d_first, 1, False)
+    run("w2_0", w_second, 2, 0)
+    run("w2_1", w_second, 2, 1)
     run("pass0", pass_on, 0, 4, 6)
     run("pass1", pass_on, 1, 5, 7)
-    run("w7", w_second, 2, 0)
-    run("d_f2", d_first, 2, False)
+    run("w2_3", w_second, 2, 3)
+    run("w2_2", w_second, 2, 2)
     run("pass2", pass_on, 2, 8)
     run("pass3", pass_on, 3, 9)
-    run("w8", w_second, 2, 1)
-    run("d_f3", d_first, 3, False)
+    run("w3_0", w_second, 3, 0)
+    run("w3_1", w_second, 3, 1)
     run("pass4", pass_on, 4, 10)
     run("pass5", pass_on, 5, 11)
+    run("w3_3", w_second, 3, 3)
+    run("w3_2", w_second, 3, 2)
+    for b in (0, 1, 3, 2):
+        run(f"d_g{b}", d_group, b)
     run("rows_in", rows_in)
-    run("w9", w_second, 3, 0)
-    run("d_f4", d_first, 4, False)
-    run("w10", w_second, 3, 1)
-    run("d_group", d_group)
-    run("w11", w_last, 0)
-    steps = [(d_second, k, b) for k in range(1, 4) for b in range(4)] + [(d_last, 0), (d_last, 1)]
-
-    def e(j):
-        run(f"e{j}", *steps[j])
-
-    for k in range(6):
-        run(f"project{k}", project, k)
-        e(k)
-    for k in range(6):
-        run(f"gate{k}", gate, k)
-        if k % 2:
-            e(6 + k // 2)
-    run("down0", down, 0)
-    e(9)
-    run("down1", down, 1)
-    run("spread0", spread, 0)
-    e(10)
-    run("down2", down, 2)
-    run("spread1", spread, 1)
-    run("relayed0", relayed, 0)
-    e(11)
-    run("down3", down, 3)
-    run("spread2", spread, 2)
-    run("relayed1", relayed, 1)
-    run("place0", place, 0)
-    e(12)
-    run("spread3", spread, 3)
-    run("relayed2", relayed, 2)
-    run("place1", place, 1)
-    e(13)
-    run("down4", down, 4)
-    run("relayed3", relayed, 3)
-    run("spread4", spread, 4)
-    run("place2", place, 2)
-    run("relayed4", relayed, 4)
-    run("place3", place, 3)
-    run("place4", place, 4)
+    run("w4_0", w_last, 0)
+    run("w4_1", w_last, 1)
+    steps = [(d_second, k, b) for k in range(1, 4) for b in (0, 1, 3, 2)] + [(d_last, 0), (d_last, 1)]
+    phases = {"p": project, "g": gate, "down": down, "spread": spread, "relayed": relayed, "place": place}
+    for name in (
+        "e0", "p0", "e1", "p1", "e2", "p2", "e3", "p3", "p4", "e4", "p5", "e5",
+        "g0", "g1", "e6", "g2", "g3", "e7", "g4", "g5",
+        "down0", "e8", "down1", "e9", "e10", "spread0", "e11", "spread1", "down2",
+        "e12", "e13", "relayed0", "spread2", "down3", "relayed1",
+        "place0", "spread3", "relayed2", "place1", "relayed3", "place2", "place3",
+    ):
+        base = name.rstrip("0123456789")
+        j = int(name[len(base) :])
+        if base == "e":
+            run(name, *steps[j])
+        else:
+            run(name, phases[base], j)
     run("last", last)
 
-    kv_copy().wait_send()
-    for k in range(6):
-        up_copy(k).wait_send()
-    for j in range(12):
-        gcopy(j).wait_send()
-    gown().wait_send()
-    rfinish()
-    for k in range(5):
-        sib_copy(k).wait_send()
-        for d in range(2):
-            x_copy(k, d).wait_send()
-            r_copy(k, d).wait_send()
-    w_finish()
-    d_finish()
+    def finish():
+        kv_copy().wait_send()
+        ref = up.at[:, pl.ds(0, 8), :]
+        remote(ref, ref, up_ss.at[0], up_rs.at[0], nxt).wait_send()
+        ref = x_all.at[pl.ds(0, 7)]
+        remote(ref, ref, g_ss.at[0], g_rs.at[0], sib).wait_send()
+        rfinish()
+        remote(f_sib, g_sib, b_ss.at[0], b_rs.at[0, 0], sib).wait_send()
+        remote(t_x, u_x, b_ss.at[1], b_rs.at[1, 0], xp).wait_send()
+        remote(t_r, u_r, b_ss.at[2], b_rs.at[2, 0], xp).wait_send()
+        w_finish()
+        d_finish()
+
+    run("finish", finish)
 
 
 def on_device(
@@ -536,6 +530,8 @@
     vmem = pl.BlockSpec(memory_space=pltpu.VMEM)
     specs = [vmem] * 14
     specs[3] = pl.BlockSpec(memory_space=pltpu.SMEM)
+    for j in (0, 1, 2, 4, 5, 9, 10, 13):
+        specs[j] = pl.BlockSpec(memory_space=pltpu.HBM)
     reduce_bufs = [
         pltpu.VMEM((4, 64, 2048), BF16),
         pltpu.VMEM((4, 64, 2048), BF16),
@@ -549,6 +545,13 @@
         in_specs=specs,
         out_specs=vmem,
         scratch_shapes=[
+            pltpu.VMEM((512, 256), BF16),
+            pltpu.VMEM((256, 2048), BF16),
+            pltpu.VMEM((64, 2048), BF16),
+            pltpu.VMEM((32, 704), BF16),
+            pltpu.VMEM((32, 704), BF16),
+            pltpu.VMEM((32, 704), BF16),
+            dma((8,)),
             pltpu.VMEM((8, 8, 2, 16, 1408), BF16),
             pltpu.VMEM((8, 8, 2, 16, 768), BF16),
             pltpu.VMEM((2, 64, 640), BF16),
@@ -565,26 +568,26 @@
             pltpu.VMEM((2, 32, 2048), BF16),
             pltpu.VMEM((8, 2, 64, 128), F32),
             pltpu.VMEM((64, 128), F32),
-            dma((2, 2, 4)),
-            dma((2, 2, 4, 2)),
-            dma((2, 2, 5)),
-            dma((2, 2, 4)),
-            dma((2, 2, 4, 4)),
-            dma((2, 2, 5)),
+            dma((4,)),
+            dma((4, 4)),
             dma((2,)),
+            dma((4,)),
+            dma((4, 4)),
+            dma((2,)),
+            dma((2,)),
+            dma((1,)),
             dma((6,)),
-            dma((6,)),
+            dma((1,)),
             dma((4,)),
-            dma((4,)),
-            dma((6,)),
-            dma((6,)),
-            dma((13,)),
-            dma((13,)),
-            dma((5, 5)),
-            dma((5, 5)),
+            dma((1,)),
+            dma((3,)),
+            dma((1,)),
+            dma((7,)),
+            dma((3,)),
+            dma((3, 4)),
         ],
         compiler_params=pltpu.CompilerParams(
-            collective_id=0, has_side_effects=True, vmem_limit_bytes=58 * 1024 * 1024
+            collective_id=0, has_side_effects=True, vmem_limit_bytes=60 * 1024 * 1024
         ),
     )(
         queries, key_states.T, value_states.T, sink_logits, out_weight, residual,

time: 94 us -> 87 us (0.926)
  Pallas kernels: 91.3 us -> 85.1 us
    pallas_call x1, Pallas kernels: 91.3 us -> 85.1 us  [on_device(): pl.pallas_call(kernel, out_shape=jax.ShapeDtypeStruct((64, 2048), BF16),...]
where the time goes in v3:
time: 87 us; the launch traced here: 86.8 us
  Pallas kernels  85.1 us (98%)
  local copies, waits for them, and re-layouts  1.67 us (2%)
    pallas_call x1, Pallas kernels, on_device(): pl.pallas_call(kernel, out_shape=jax.ShapeDtypeStruct((64, 2048), BF16),...  85.1 us

profile of v3, /device:TPU:1, one launch (start us, length us, event | category | flops | bytes accessed | tf_op | source)
XLA Modules:
  0.0 86.8 jit_solution(8110034935321459759)
XLA Ops:
  0.0 85.1 %shard_map.136 = bf16[64,2048]{1,0:T(8,128)(2,1)} custom-call(bf16[512,256]{1,0:T(8,128)(2,1)} %q_hbm.1, bf16[64,512]{1,0:T(8,128)(2,1)} %bitcast.6, bf16[64,512]{1,0:T(8,128)(2,1)} %bitcast.7, f32[4]{0:T(128)} %sink_ref.1, bf16[256,2048]{1,0:T(8,128)(2,1)} %ow_hbm.1, bf16[64,2048]{1,0:T(8,128)(2,1)} %res_hbm.1, f32[1,2048]{1,0:T(1,128)} %bitcast.9, ...), custom_call_target="tpu_custom_call" | custom-call | tf_op jit(solution)/shard_map/pallas_call | solution.py:542
  85.1 1.7 %copy.16 = bf16[64,2048]{1,0:T(8,128)(2,1)} copy(bf16[64,2048]{1,0:T(8,128)(2,1)} %shard_map.136) | data formatting | bytes 524288
